TPU v7x, 32 devices: a whole 2x2x4 slice. The times are simulated.
32 devices in a mesh: fs: 8 (over z, x), tp: 4 (over y, core).
Axes of the slice: x: 2, y: 2, z: 4, core: 2. Of those that a mesh axis runs over, the one named last changes fastest.
Arguments:
- tokens: bfloat16 [8192, 2048], P(('fs', 'tp')), may hold values from -6 to 6
- mix_gain: float32 [2048], replicated, may hold values from 0.1 to 1.9
- ffn_gain: float32 [2048], replicated, may hold values from 0.1 to 1.9
- u_weight: float32 [2048, 2048], P('fs', 'tp'), may hold values from -0.125 to 0.125
- u_scale: float32 [2048], P('tp'), may hold values from 0.5 to 2
- v_weight: float32 [2048, 2048], P('fs', 'tp'), may hold values from -0.125 to 0.125
- v_scale: float32 [2048], P('tp'), may hold values from 0.3 to 12
- v_gain: float32 [2048], P('tp'), may hold values from 0.1 to 1.9
- spatial_weight: bfloat16 [8, 128, 128], replicated, may hold values from -0.5 to 0.5
- spatial_bias: float32 [8, 128], replicated, may hold values from 0.1 to 1.9
- out_weight: float32 [2048, 2048], P('tp', 'fs'), may hold values from -0.125 to 0.125
- out_scale: float32 [2048], P('fs'), may hold values from 0.5 to 2
- gate_weight: float32 [2048, 6144], P('fs', 'tp'), may hold values from -0.125 to 0.125
- gate_scale: float32 [6144], P('tp'), may hold values from 0.5 to 2
- up_weight: float32 [2048, 6144], P('fs', 'tp'), may hold values from -0.125 to 0.125
- up_scale: float32 [6144], P('tp'), may hold values from 0.5 to 2
- down_weight: float32 [6144, 2048], P('tp', 'fs'), may hold values from -0.078125 to 0.078125
- down_scale: float32 [2048], P('fs'), may hold values from 0.5 to 2
Outputs:
- layer_out: bfloat16 [8192, 2048], P(('fs', 'tp'))
All inputs are finite; a program needn't handle non-finite values.
Results may differ from a plain program's by a relative error of at most 0.02.
Values may be sent and summed in bfloat16 or wider, within the bound.
A program may use at most 128 MiB of HBM per device.

v0:
```python
import jax
import jax.numpy as jnp
from jax import lax
from jax.sharding import PartitionSpec as P

A = 2048
A_GROUPS = 8
BLK = 128


def rms_rows(values, norm_gain):
    widened = values.astype(jnp.float32)
    factor = lax.rsqrt(jnp.mean(widened * widened, axis=1, keepdims=True) + 1e-06)
    return (widened * factor * norm_gain).astype(jnp.bfloat16)


def collect_rows(shard_rows, project):
    return project(lax.all_gather(shard_rows, "tp", axis=0, tiled=True), jnp.int32(0))


def reduce_rows(term_fn, local_rows):
    return lax.psum_scatter(
        term_fn(jnp.int32(0), lax.axis_size("tp") * local_rows).astype(jnp.bfloat16),
        "tp",
        scatter_dimension=0,
        tiled=True,
    ).astype(jnp.float32)


def local(
    tokens,
    mix_gain,
    ffn_gain,
    u_weight,
    u_scale,
    v_weight,
    v_scale,
    v_gain,
    spatial_weight,
    spatial_bias,
    out_weight,
    out_scale,
    gate_weight,
    gate_scale,
    up_weight,
    up_scale,
    down_weight,
    down_scale,
):
    local_rows = tokens.shape[0]
    out_columns, down_columns = (
        lax.all_gather(out_scale, "fs", axis=0, tiled=True),
        lax.all_gather(down_scale, "fs", axis=0, tiled=True),
    )
    u_whole, v_whole, out_whole, gate_whole, up_whole, down_whole = (
        lax.all_gather(u_weight.astype(jnp.bfloat16), "fs", axis=0, tiled=True),
        lax.all_gather(v_weight.astype(jnp.bfloat16), "fs", axis=0, tiled=True),
        lax.all_gather(out_weight.astype(jnp.bfloat16), "fs", axis=1, tiled=True),
        lax.all_gather(gate_weight.astype(jnp.bfloat16), "fs", axis=0, tiled=True),
        lax.all_gather(up_weight.astype(jnp.bfloat16), "fs", axis=0, tiled=True),
        lax.all_gather(down_weight.astype(jnp.bfloat16), "fs", axis=1, tiled=True),
    )
    normed = rms_rows(tokens, mix_gain)

    def project_mixer(segment, offset):
        u_pre = jnp.dot(segment, u_whole, preferred_element_type=jnp.float32) * u_scale
        v_pre = jnp.dot(segment, v_whole, preferred_element_type=jnp.float32) * v_scale
        return jnp.concatenate(
            [jax.nn.gelu(u_pre, approximate=True), jax.nn.gelu(v_pre, approximate=True)], axis=1
        ).astype(jnp.bfloat16)

    joined = collect_rows(normed, project_mixer)
    columns = u_whole.shape[1]
    u_values = joined[:, :columns]
    v_wide = joined[:, columns:].astype(jnp.float32)
    totals, squares = lax.psum((jnp.sum(v_wide, axis=1), jnp.sum(v_wide * v_wide, axis=1)), "tp")
    average = totals / A
    spread = squares / A - average * average
    v_normed = ((v_wide - average[:, None]) * lax.rsqrt(spread + 1e-05)[:, None] * v_gain).astype(
        jnp.bfloat16
    )
    group_dim = A // A_GROUPS
    groups = columns // group_dim
    first_group = lax.axis_index("tp") * groups
    weights = lax.dynamic_slice_in_dim(spatial_weight, first_group, groups, 0)
    offsets = lax.dynamic_slice_in_dim(spatial_bias, first_group, groups, 0)
    causal = jnp.tril(jnp.ones((BLK, BLK), dtype=bool))
    masked = jnp.where(causal[None], weights, jnp.zeros_like(weights))
    blocks = v_normed.reshape(-1, BLK, groups, group_dim)
    mixed_sum = jnp.einsum("gts,bsgd->btgd", masked, blocks, preferred_element_type=jnp.float32)
    mixed_sum = mixed_sum + offsets.T[None, :, :, None]
    gated_rows = (u_values.reshape(blocks.shape).astype(jnp.float32) * mixed_sum).astype(
        jnp.bfloat16
    )
    gated_rows = gated_rows.reshape(-1, columns)

    def mixer_term(offset, amount):
        return jnp.dot(gated_rows, out_whole, preferred_element_type=jnp.float32) * out_columns

    residual = (tokens.astype(jnp.float32) + reduce_rows(mixer_term, local_rows)).astype(
        jnp.bfloat16
    )
    normed_second = rms_rows(residual, ffn_gain)

    def project_ffn(segment, offset):
        gate_pre = jnp.dot(segment, gate_whole, preferred_element_type=jnp.float32) * gate_scale
        up_pre = jnp.dot(segment, up_whole, preferred_element_type=jnp.float32) * up_scale
        return (jax.nn.silu(gate_pre) * up_pre).astype(jnp.bfloat16)

    hidden = collect_rows(normed_second, project_ffn)

    def ffn_term(offset, amount):
        return jnp.dot(hidden, down_whole, preferred_element_type=jnp.float32) * down_columns

    return (residual.astype(jnp.float32) + reduce_rows(ffn_term, local_rows)).astype(jnp.bfloat16)


def solution(mesh):
    placed = (
        P(("fs", "tp"), None),
        P(),
        P(),
        P("fs", "tp"),
        P("tp"),
        P("fs", "tp"),
        P("tp"),
        P("tp"),
        P(),
        P(),
        P("tp", "fs"),
        P("fs"),
        P("fs", "tp"),
        P("tp"),
        P("fs", "tp"),
        P("tp"),
        P("tp", "fs"),
        P("fs"),
    )
    return jax.shard_map(
        local, mesh=mesh, in_specs=placed, out_specs=P(("fs", "tp"), None), check_vma=False
    )
```

profile of v0, /device:TPU:0, one launch (start us, length us, event | category | flops | bytes accessed | tf_op | source)
XLA Modules:
  0.0 656.6 jit_solution(5270120001855594099)
XLA Ops:
  6.5 1.9 convert_element_type.74
  13.1 22.4 %all-gather = f32[8,1,256]{2,1,0:T(1,128)S(1)} all-gather(f32[1,1,256]{2,1,0:T(1,128)S(1)} %bitcast.46), channel_id=1, replica_groups=mesh['fs'=8,'tp'=4] {'fs'}, dimensions={0}, use_global_device_ids=true | all-gather | bytes 9216 | tf_op jit(solution)/shard_map/all_gather | solution.py:52
  35.6 25.9 %all-gather.15.cloned.1.call-done = bf16[2048,512]{1,0:T(8,128)(2,1)} async-done(((bf16[256,512]{1,0:T(8,128)(2,1)}), bf16[2048,512]{1,0:T(8,128)(2,1)}) %all-gather.15.cloned.1.call-update) | async-done | bytes 2097168 | tf_op jit(solution)/shard_map/all_gather | solution.py:57
  61.4 34.6 %all-gather.11.cloned.1.call-done = bf16[1024,2048]{1,0:T(8,128)(2,1)} async-done(((bf16[256,2048]{1,0:T(8,128)(2,1)}), bf16[1024,2048]{1,0:T(8,128)(2,1)}) %all-gather.11.cloned.1.call-update) | async-done | bytes 4194320 | tf_op jit(solution)/shard_map/all_gather | solution.py:18
  96.0 6.0 convert_reduce_fusion
  102.0 6.0 all-reduce
  109.5 37.7 %all-gather.13.cloned.1.call-done = bf16[2048,512]{1,0:T(8,128)(2,1)} async-done(((bf16[256,512]{1,0:T(8,128)(2,1)}), bf16[2048,512]{1,0:T(8,128)(2,1)}) %all-gather.13.cloned.1.call-update) | async-done | bytes 2097168 | tf_op jit(solution)/shard_map/all_gather | solution.py:56
  147.2 5.6 fusion.30
  152.9 2.3 reshape.46
  155.2 2.7 copy.28
  160.5 37.6 %all-gather.17.cloned.1.call-done = bf16[512,2048]{1,0:T(8,128)(2,1)} async-done(((bf16[512,256]{1,0:T(8,128)(2,1)}), bf16[512,2048]{1,0:T(8,128)(2,1)}) %all-gather.17.cloned.1.call-update) | async-done | bytes 2097168 | tf_op jit(solution)/shard_map/all_gather | solution.py:58
  198.1 6.0 multiply_convert_fusion.1
  206.6 40.5 %reduce-scatter.3.cloned.1.call-done = bf16[256,2048]{1,0:T(8,128)(2,1)} async-done(((bf16[1024,2048]{1,0:T(8,128)(2,1)}), bf16[256,2048]{1,0:T(8,128)(2,1)}) %reduce-scatter.3.cloned.1.call-update) | async-done | bytes 1048592 | tf_op jit(solution)/shard_map/reduce_scatter | solution.py:22
  250.5 2.5 convert_element_type.85
  253.1 2.4 convert_element_type.87
  255.5 21.3 %all-gather.1 = f32[8,1,256]{2,1,0:T(1,128)S(1)} all-gather(f32[1,1,256]{2,1,0:T(1,128)S(1)} %bitcast.47), channel_id=1, replica_groups=mesh['fs'=8,'tp'=4] {'fs'}, dimensions={0}, use_global_device_ids=true | all-gather | bytes 9216 | tf_op jit(solution)/shard_map/all_gather | solution.py:53
  276.8 71.0 %all-gather.21.cloned.1.call-done = bf16[2048,1536]{1,0:T(8,128)(2,1)} async-done(((bf16[256,1536]{1,0:T(8,128)(2,1)}), bf16[2048,1536]{1,0:T(8,128)(2,1)}) %all-gather.21.cloned.1.call-update) | async-done | bytes 6291472 | tf_op jit(solution)/shard_map/all_gather | solution.py:59
  347.9 34.2 %all-gather.19.cloned.1.call-done = bf16[1024,2048]{1,0:T(8,128)(2,1)} async-done(((bf16[256,2048]{1,0:T(8,128)(2,1)}), bf16[1024,2048]{1,0:T(8,128)(2,1)}) %all-gather.19.cloned.1.call-update) | async-done | bytes 4194320 | tf_op jit(solution)/shard_map/all_gather | solution.py:18
  382.1 11.7 %fusion.41 = f32[1024,1536]{1,0:T(8,128)} fusion(bf16[1024,2048]{1,0:T(8,128)(2,1)} %all-gather.19.cloned.1.call-done, bf16[2048,1536]{1,0:T(8,128)(2,1)} %all-gather.21.cloned.1.call-done), kind=kOutput, calls=%fused_computation.62 | convolution fusion | flops 6442450944 | bytes 16777216 | tf_op jit(solution)/shard_map/dot_general | solution.py:106
  393.8 89.2 %all-gather.23.cloned.1.call-done = bf16[2048,1536]{1,0:T(8,128)(2,1)} async-done(((bf16[256,1536]{1,0:T(8,128)(2,1)}), bf16[2048,1536]{1,0:T(8,128)(2,1)}) %all-gather.23.cloned.1.call-update) | async-done | bytes 6291472 | tf_op jit(solution)/shard_map/all_gather | solution.py:60
  483.0 99.7 %all-gather.25.cloned.1.call-done = bf16[1536,2048]{1,0:T(8,128)(2,1)} async-done(((bf16[1536,256]{1,0:T(8,128)(2,1)}), bf16[1536,2048]{1,0:T(8,128)(2,1)}) %all-gather.25.cloned.1.call-update) | async-done | bytes 6291472 | tf_op jit(solution)/shard_map/all_gather | solution.py:61
  582.7 21.4 %multiply_convert_fusion = bf16[1024,2048]{1,0:T(8,128)(2,1)} fusion(bf16[1536,2048]{1,0:T(8,128)(2,1)} %all-gather.25.cloned.1.call-done, f32[2048]{0:T(1024)S(1)} %bitcast.45, f32[1024,1536]{1,0:T(8,128)} %fusion.41, bf16[1024,2048]{1,0:T(8,128)(2,1)} %all-gather.19.cloned.1.call-done, bf16[2048,1536]{1,0:T(8,128)(2,1)} %all-gather.23.cloned.1.call-done, ...), kind=kOutput, calls=%fused_computation | convolution fusion | flops 12901679104 | bytes 27283456 | tf_op jit(solution)/shard_map/dot_general | solution.py:113
  604.1 42.9 %reduce-scatter.5.cloned.1.call-done = bf16[256,2048]{1,0:T(8,128)(2,1)} async-done(((bf16[1024,2048]{1,0:T(8,128)(2,1)}), bf16[256,2048]{1,0:T(8,128)(2,1)}) %reduce-scatter.5.cloned.1.call-update) | async-done | bytes 1048592 | tf_op jit(solution)/shard_map/reduce_scatter | solution.py:22
  647.1 2.7 fusion.27
  (68 shorter events, 14.7 us)
Async XLA Ops:
  6.5 29.0 %copy-start = (f32[8,128]{1,0:T(8,128)S(1)}, f32[8,128]{1,0:T(8,128)}, u32[]{:S(2)}) copy-start(f32[8,128]{1,0:T(8,128)} %param.27) | copy-start | bytes 12292
  6.5 3.5 copy-start.2
  6.5 3.5 copy-start.7
  6.5 54.9 %all-gather.15.cloned.1.call-start = ((), (), s32[]{:S(2)}) async-start(), calls=%async_computation.4 | async-start | bytes 2359296 | tf_op jit(solution)/shard_map/all_gather | solution.py:57
  8.4 3.0 copy-start.5
  8.4 87.5 %all-gather.11.cloned.1.call-start = ((), (), s32[]{:S(2)}) async-start(), calls=%async_computation.2 | async-start | bytes 5242880 | tf_op jit(solution)/shard_map/all_gather | solution.py:18
  10.1 2.2 copy-start.6
  11.4 84.6 %copy-start.14 = (f32[512]{0:T(512)S(1)}, f32[512]{0:T(512)}, u32[]{:S(2)}) copy-start(f32[512]{0:T(512)} %param.24) | copy-start | bytes 6148
  11.4 135.8 %all-gather.13.cloned.1.call-start = ((), (), s32[]{:S(2)}) async-start(), calls=%async_computation.3 | async-start | bytes 2359296 | tf_op jit(solution)/shard_map/all_gather | solution.py:56
  12.2 185.8 %all-gather.17.cloned.1.call-start = ((), (), s32[]{:S(2)}) async-start(), calls=%async_computation.5 | async-start | bytes 2359296 | tf_op jit(solution)/shard_map/all_gather | solution.py:58
  13.0 234.0 %reduce-scatter.3.cloned.1.call-start = ((), (), s32[]{:S(2)}) async-start(), calls=%async_computation.6 | async-start | bytes 5242880 | tf_op jit(solution)/shard_map/reduce_scatter | solution.py:22
  35.5 72.4 %copy-start.9 = (f32[512]{0:T(512)S(1)}, f32[512]{0:T(512)}, u32[]{:S(2)}) copy-start(f32[512]{0:T(512)} %param.25) | copy-start | bytes 6148
  108.0 39.2 %copy-start.15 = (f32[512]{0:T(512)S(1)}, f32[512]{0:T(512)}, u32[]{:S(2)}) copy-start(f32[512]{0:T(512)} %param.22) | copy-start | bytes 6148
  204.1 44.7 %copy-start.8 = (f32[2048]{0:T(1024)S(1)}, f32[2048]{0:T(1024)}, u32[]{:S(2)}) copy-start(f32[2048]{0:T(1024)} %param.20) | copy-start | bytes 24580
  204.1 143.7 %all-gather.21.cloned.1.call-start = ((), (), s32[]{:S(2)}) async-start(), calls=%async_computation.8 | async-start | bytes 7077888 | tf_op jit(solution)/shard_map/all_gather | solution.py:59
  206.5 175.6 %all-gather.19.cloned.1.call-start = ((), (), s32[]{:S(2)}) async-start(), calls=%async_computation.7 | async-start | bytes 5242880 | tf_op jit(solution)/shard_map/all_gather | solution.py:18
  247.0 1.8 copy-start.3
  250.3 232.7 %all-gather.23.cloned.1.call-start = ((), (), s32[]{:S(2)}) async-start(), calls=%async_computation.9 | async-start | bytes 7077888 | tf_op jit(solution)/shard_map/all_gather | solution.py:60
  253.0 2.5 copy-start.11
  253.0 329.7 %all-gather.25.cloned.1.call-start = ((), (), s32[]{:S(2)}) async-start(), calls=%async_computation.10 | async-start | bytes 7077888 | tf_op jit(solution)/shard_map/all_gather | solution.py:61
  255.5 391.6 %reduce-scatter.5.cloned.1.call-start = ((), (), s32[]{:S(2)}) async-start(), calls=%async_computation.11 | async-start | bytes 5242880 | tf_op jit(solution)/shard_map/reduce_scatter | solution.py:22
  276.8 305.9 %copy-start.12 = (f32[1536]{0:T(1024)S(1)}, f32[1536]{0:T(1024)}, u32[]{:S(2)}) copy-start(f32[1536]{0:T(1024)} %param.33) | copy-start | bytes 18436
  276.8 305.9 %copy-start.13 = (f32[1536]{0:T(1024)S(1)}, f32[1536]{0:T(1024)}, u32[]{:S(2)}) copy-start(f32[1536]{0:T(1024)} %param.31) | copy-start | bytes 18436
  604.1 45.7 %copy-start.1 = (f32[8,128]{1,0:T(8,128)S(1)}, f32[8,128]{1,0:T(8,128)}, u32[]{:S(2)}) copy-start(f32[8,128]{1,0:T(8,128)} %param.27) | copy-start | bytes 12292
  (2 other events, 3.1 us)
Sparse Core Ops, SparseCore 0:
  9.5 51.9 all-gather.14
  63.0 32.9 all-gather.10
  98.1 49.0 all-gather.12
  149.1 48.8 all-gather.16
  204.2 42.7 reduce-scatter.2
  249.1 98.7 all-gather.20
  349.4 32.6 all-gather.18
  384.3 98.6 all-gather.22
  485.0 97.6 all-gather.24
  604.2 42.7 reduce-scatter.4
where the time goes:
time: 657 us
  waiting for transfers between devices  513 us (78%)
  matrix products  52.5 us (8%)
  blocking collectives  49.7 us (8%)
  other arithmetic  18.4 us (3%)
  between operations  13.7 us (2%)
  local copies, waits for them, and re-layouts  8.27 us (1%)
    all_gather x1, waiting for transfers between devices, local(): lax.all_gather(down_weight.astype(jnp.bfloat16), 'fs', axis=1, tiled=True)  99.7 us
    all_gather x1, waiting for transfers between devices, local(): lax.all_gather(up_weight.astype(jnp.bfloat16), 'fs', axis=0, tiled=True)  89.2 us
    reduce_scatter x2, waiting for transfers between devices, reduce_rows(): lax.psum_scatter(term_fn(jnp.int32(0), lax.axis_size('tp') * local_rows)....  83.4 us
    all_gather x1, waiting for transfers between devices, local(): lax.all_gather(gate_weight.astype(jnp.bfloat16), 'fs', axis=0, tiled=True)  71 us
    all_gather x2, waiting for transfers between devices, collect_rows(): lax.all_gather(shard_rows, 'tp', axis=0, tiled=True)  68.8 us
    all_gather x1, waiting for transfers between devices, local(): lax.all_gather(u_weight.astype(jnp.bfloat16), 'fs', axis=0, tiled=True)  37.7 us
    all_gather x1, waiting for transfers between devices, local(): lax.all_gather(out_weight.astype(jnp.bfloat16), 'fs', axis=1, tiled=True)  37.6 us
    all_gather x1, waiting for transfers between devices, local(): lax.all_gather(v_weight.astype(jnp.bfloat16), 'fs', axis=0, tiled=True)  25.9 us
  transfers between devices with their start and end apart: 10, of which 10 were waited for; matrix products, arithmetic and copies ran while one was open for 7% of the time, Pallas kernels for 0%

commit v1 on v0

v1 whole, which is shorter than its diff:
```python
import functools
import jax
import jax.numpy as jnp
from jax import lax
from jax.experimental import pallas as pl
from jax.experimental.pallas import tpu as pltpu
from jax.sharding import PartitionSpec as P

A_GROUPS = 8
BLK = 128
UV, OUT, GATE, UP, DOWN = range(5)
BF = jnp.bfloat16
F32 = jnp.float32


def rms(values, gain):
    wide = values.astype(F32)
    factor = lax.rsqrt(jnp.mean(wide * wide, axis=1, keepdims=True) + 1e-06)
    return (wide * factor * gain).astype(BF)


def kernel(
    nf, nt, nz, nx,
    tokens, mix_gain, ffn_gain, uv_scale, v_gain, mixers, offsets, gate_scale, up_scale,
    uv_in, out_in, gate_in, up_in, down_in,
    result,
    w_uv, w_out, w_gate, w_up, w_down, rows_all, uvals, vvals, gated, hidden,
    staged, landed, stats, residual,
    own_sem, w_recv, w_send, row_recv, row_send, stat_recv, stat_send, part_recv, part_send,
):
    fs, tp = lax.axis_index("fs"), lax.axis_index("tp")
    coord = {"z": fs // nx, "x": fs % nx}
    size = {"z": nz, "x": nx}
    stride = {"z": nx, "x": 1}
    order = {m: ("z", "x") for m in range(5)}
    local = tokens.shape[0]
    total = rows_all.shape[0]
    width = tokens.shape[1]
    cols = uvals.shape[1]
    sources = (uv_in, out_in, gate_in, up_in, down_in)
    whole = (w_uv, w_out, w_gate, w_up, w_down)

    def slot(m, s):
        if m in (OUT, DOWN):
            return whole[m].at[s]
        depth = sources[m].shape[0]
        return whole[m].at[pl.ds(pl.multiple_of(s * depth, depth), depth)]

    def reaches(axis, d):
        return coord[axis] + d < size[axis] if d > 0 else coord[axis] > 0

    pending = []

    def copy_of(m, s, axis, d):
        lane = (0 if axis == "z" else 2) + (0 if d > 0 else 1)
        return pltpu.make_async_remote_copy(
            src_ref=slot(m, s), dst_ref=slot(m, s),
            send_sem=w_send.at[m, s, lane], recv_sem=w_recv.at[m, s],
            device_id={"fs": fs + d * stride[axis], "tp": tp},
            device_id_type=pl.DeviceIdType.MESH,
        )

    def send(m, s, axis, d, valid):
        allowed = jnp.logical_and(valid, reaches(axis, d))

        @pl.when(allowed)
        def _():
            copy_of(m, s, axis, d).start()

        pending.append((allowed, m, s, axis, d))

    def own(m, axis):
        if size[axis] > 1:
            for d in (1, -1):
                send(m, fs, axis, d, fs >= 0)

    def arrived(m, s, axis, d, valid):
        @pl.when(valid)
        def _():
            copy_of(m, s, axis, -d).wait_recv()

    def first_line(m, then=None):
        p, q = order[m]
        for t in range(1, size[p]):
            for d in (1, -1):
                at = coord[p] - d * t
                valid = jnp.logical_and(at >= 0, at < size[p])
                s = jnp.where(valid, fs - d * t * stride[p], fs)
                arrived(m, s, p, d, valid)
                if t < size[p] - 1:
                    send(m, s, p, d, valid)
                if size[q] > 1:
                    for e in (1, -1):
                        send(m, s, q, e, valid)
                if then:
                    pl.when(valid)(functools.partial(then, s))

    def second_line(m, then=None):
        p, q = order[m]
        for k in range(size[p]):
            for sign in (1, -1) if k else (1,):
                there = coord[p] + sign * k
                inside = jnp.logical_and(there >= 0, there < size[p])
                for t in range(1, size[q]):
                    for d in (1, -1):
                        at = coord[q] - d * t
                        valid = jnp.logical_and(inside, jnp.logical_and(at >= 0, at < size[q]))
                        s = jnp.where(valid, fs + sign * k * stride[p] - d * t * stride[q], fs)
                        arrived(m, s, q, d, valid)
                        if t < size[q] - 1:
                            send(m, s, q, d, valid)
                        if then:
                            pl.when(valid)(functools.partial(then, s))

    mine = [pltpu.make_async_copy(sources[m], slot(m, fs), own_sem.at[m]) for m in range(5)]
    for copy in mine:
        copy.start()
    mine[UV].wait()
    own(UV, "z")
    own(UV, "x")

    def peer_of(j):
        return lax.rem(tp + j, nt)

    def row_copy(phase, j, owner):
        part = rows_all.at[pl.ds(pl.multiple_of(owner * local, local), local)]
        return pltpu.make_async_remote_copy(
            src_ref=part, dst_ref=part,
            send_sem=row_send.at[phase, j], recv_sem=row_recv.at[phase, owner],
            device_id={"fs": fs, "tp": peer_of(j)}, device_id_type=pl.DeviceIdType.MESH,
        )

    def stat_copy(j, owner):
        return pltpu.make_async_remote_copy(
            src_ref=stats.at[owner], dst_ref=stats.at[owner],
            send_sem=stat_send.at[j], recv_sem=stat_recv.at[owner],
            device_id={"fs": fs, "tp": peer_of(j)}, device_id_type=pl.DeviceIdType.MESH,
        )

    def part_copy(phase, j, owner, s):
        peer = peer_of(j)
        return pltpu.make_async_remote_copy(
            src_ref=staged.at[s, pl.ds(pl.multiple_of(peer * local, local), local)],
            dst_ref=landed.at[owner, s],
            send_sem=part_send.at[phase, j, s], recv_sem=part_recv.at[phase, owner, s],
            device_id={"fs": fs, "tp": peer}, device_id_type=pl.DeviceIdType.MESH,
        )

    step = min(64, local)

    def norm_rows(source, gain):
        @pl.loop(0, local // step)
        def _(i):
            here = pl.ds(pl.multiple_of(i * step, step), step)
            there = pl.ds(pl.multiple_of(tp * local + i * step, step), step)
            rows_all[there, :] = rms(source[here, :], gain[...])

    norm_rows(tokens, mix_gain)
    for j in range(1, nt):
        row_copy(0, j, tp).start()
    mine[OUT].wait()
    own(OUT, "x")
    own(OUT, "z")
    mine[GATE].wait()
    own(GATE, "x")
    first_line(UV)
    own(GATE, "z")
    mine[UP].wait()
    own(UP, "x")
    second_line(UV)
    for j in range(1, nt):
        row_copy(0, j, peer_of(j)).wait_recv()

    tile = 256
    stat_rows = BLK

    @pl.loop(0, total // tile)
    def _(i):
        here = pl.ds(pl.multiple_of(i * tile, tile), tile)
        for c in range(2 * cols // tile):
            at = slice(c * tile, (c + 1) * tile)
            pre = jnp.dot(rows_all[here, :], w_uv[:, at], preferred_element_type=F32)
            value = jax.nn.gelu(pre * uv_scale[:, at], approximate=True).astype(BF)
            if c * tile < cols:
                uvals[here, at] = value
            else:
                vvals[here, c * tile - cols:(c + 1) * tile - cols] = value

    lanes = lax.broadcasted_iota(jnp.int32, (stat_rows, 128), 1)

    @pl.loop(0, total // stat_rows)
    def _(i):
        here = pl.ds(pl.multiple_of(i * stat_rows, stat_rows), stat_rows)
        wide = vvals[here, :].astype(F32)
        sums = jnp.sum(wide, axis=1, keepdims=True)
        squares = jnp.sum(wide * wide, axis=1, keepdims=True)
        both = jnp.where(lanes == 0, sums, jnp.where(lanes == 1, squares, 0.0))
        stats[tp, :, here] = both.T[0:8, :]

    for j in range(1, nt):
        stat_copy(j, tp).start()
    first_line(OUT)
    own(UP, "z")
    mine[DOWN].wait()
    own(DOWN, "x")
    second_line(OUT)
    for j in range(1, nt):
        stat_copy(j, peer_of(j)).wait_recv()

    group_dim = (cols * nt) // A_GROUPS

    @pl.loop(0, total // BLK)
    def _(i):
        here = pl.ds(pl.multiple_of(i * BLK, BLK), BLK)
        summed = stats[0, :, here]
        for t in range(1, nt):
            summed = summed + stats[t, :, here]
        turned = jnp.concatenate([summed] * (BLK // 8), axis=0).T
        average = turned[:, 0:1] / (cols * nt)
        spread = turned[:, 1:2] / (cols * nt) - average * average
        wide = vvals[here, :].astype(F32)
        normed = ((wide - average) * lax.rsqrt(spread + 1e-05) * v_gain[...]).astype(BF)
        for g in range(cols // group_dim):
            at = slice(g * group_dim, (g + 1) * group_dim)
            mixed = jnp.dot(mixers[g], normed[:, at], preferred_element_type=F32)
            mixed = mixed + offsets[:, g:g + 1]
            gated[here, at] = (uvals[here, at].astype(F32) * mixed).astype(BF)

    def product(phase, left, matrix, s):
        part = min(512, total)

        @pl.loop(0, total // part)
        def _(i):
            here = pl.ds(pl.multiple_of(i * part, part), part)
            staged[s, here, :] = jnp.dot(
                left[here, :], matrix[s], preferred_element_type=F32
            ).astype(BF)

        for j in range(1, nt):
            part_copy(phase, j, tp, s).start()

    @pl.loop(0, nf)
    def _(s):
        product(0, gated, w_out, s)

    first_line(GATE)
    own(DOWN, "z")

    block = staged.shape[2]

    def collect(phase, base, target):
        for s in range(nf):
            for j in range(1, nt):
                part_copy(phase, j, peer_of(j), s).wait_recv()
            at = slice(s * block, (s + 1) * block)
            summed = staged[s, pl.ds(pl.multiple_of(tp * local, local), local), :].astype(F32)
            for j in range(1, nt):
                summed = summed + landed[peer_of(j), s].astype(F32)
            target[:, at] = (base[:, at].astype(F32) + summed).astype(BF)

    collect(0, tokens, residual)
    for j in range(1, nt):
        row_copy(0, j, tp).wait_send()
    norm_rows(residual, ffn_gain)
    for j in range(1, nt):
        row_copy(1, j, tp).start()

    @pl.loop(0, nf)
    def _(s):
        for j in range(1, nt):
            part_copy(0, j, tp, s).wait_send()

    first_line(UP)
    second_line(GATE)
    for j in range(1, nt):
        row_copy(1, j, peer_of(j)).wait_recv()
    first_line(DOWN)
    second_line(UP)
    hidden_cols = hidden.shape[1]

    @pl.loop(0, hidden_cols // tile)
    def _(c):
        at = pl.ds(pl.multiple_of(c * tile, tile), tile)

        @pl.loop(0, total // tile)
        def _(i):
            here = pl.ds(pl.multiple_of(i * tile, tile), tile)
            gate = jnp.dot(rows_all[here, :], w_gate[:, at], preferred_element_type=F32)
            gate = gate * gate_scale[:, at]
            up = jnp.dot(rows_all[here, :], w_up[:, at], preferred_element_type=F32)
            up = up * up_scale[:, at]
            hidden[here, at] = (gate / (1.0 + jnp.exp(-gate)) * up).astype(BF)

    for k in range(nz):
        for sign in (1, -1) if k else (1,):
            there = coord["z"] + sign * k
            inside = jnp.logical_and(there >= 0, there < nz)

            @pl.when(inside)
            def _():
                product(1, hidden, w_down, fs + sign * k * nx)

    second_line(DOWN, lambda s: product(1, hidden, w_down, s))
    collect(1, residual, result)
    for j in range(1, nt):
        row_copy(1, j, tp).wait_send()
        stat_copy(j, tp).wait_send()

    @pl.loop(0, nf)
    def _(s):
        for j in range(1, nt):
            part_copy(1, j, tp, s).wait_send()

    for allowed, m, s, axis, d in pending:
        pl.when(allowed)(lambda: copy_of(m, s, axis, d).wait_send())


def layer(
    nf, nt,
    tokens, mix_gain, ffn_gain, u_weight, u_scale, v_weight, v_scale, v_gain,
    spatial_weight, spatial_bias, out_weight, out_scale, gate_weight, gate_scale,
    up_weight, up_scale, down_weight, down_scale,
):
    nz = max(n for n in (1, 2, 4) if nf % n == 0)
    nx = nf // nz
    local, width = tokens.shape
    total = local * nt
    cols, ff = u_weight.shape[1], gate_weight.shape[1]
    groups = A_GROUPS // nt
    first = lax.axis_index("tp") * groups
    causal = jnp.tril(jnp.ones((BLK, BLK), dtype=bool))
    mixers = lax.dynamic_slice_in_dim(spatial_weight, first, groups, 0)
    mixers = jnp.where(causal[None], mixers, jnp.zeros_like(mixers))
    offsets = lax.dynamic_slice_in_dim(spatial_bias, first, groups, 0).T
    uv = jnp.concatenate([u_weight.astype(BF), v_weight.astype(BF)], axis=1)
    uv_scale = jnp.concatenate([u_scale, v_scale])[None]
    out = (out_weight * out_scale[None]).astype(BF)
    down = (down_weight * down_scale[None]).astype(BF)
    block = out.shape[1]
    vmem = pl.BlockSpec(memory_space=pltpu.VMEM)
    hbm = pl.BlockSpec(memory_space=pl.ANY)
    dma = pltpu.SemaphoreType.DMA
    return pl.pallas_call(
        functools.partial(kernel, nf, nt, nz, nx),
        out_shape=jax.ShapeDtypeStruct((local, width), BF),
        in_specs=[vmem] * 9 + [hbm] * 5,
        out_specs=vmem,
        scratch_shapes=[
            pltpu.VMEM((width, 2 * cols), BF),
            pltpu.VMEM((nf,) + out.shape, BF),
            pltpu.VMEM((width, ff), BF),
            pltpu.VMEM((width, ff), BF),
            pltpu.VMEM((nf,) + down.shape, BF),
            pltpu.VMEM((total, width), BF),
            pltpu.VMEM((total, cols), BF),
            pltpu.VMEM((total, cols), BF),
            pltpu.VMEM((total, cols), BF),
            pltpu.VMEM((total, ff), BF),
            pltpu.VMEM((nf, total, block), BF),
            pltpu.VMEM((nt, nf, local, block), BF),
            pltpu.VMEM((nt, 8, total), F32),
            pltpu.VMEM((local, width), BF),
            dma((5,)), dma((5, nf)), dma((5, nf, 4)),
            dma((2, nt)), dma((2, nt)), dma((nt,)), dma((nt,)),
            dma((2, nt, nf)), dma((2, nt, nf)),
        ],
        compiler_params=pltpu.CompilerParams(
            has_side_effects=True, vmem_limit_bytes=67043328
        ),
    )(
        tokens, mix_gain[None], ffn_gain[None], uv_scale, v_gain[None], mixers, offsets,
        gate_scale[None], up_scale[None],
        uv, out, gate_weight.astype(BF), up_weight.astype(BF), down,
    )


def solution(mesh):
    placed = (
        P(("fs", "tp"), None), P(), P(),
        P("fs", "tp"), P("tp"), P("fs", "tp"), P("tp"), P("tp"), P(), P(),
        P("tp", "fs"), P("fs"), P("fs", "tp"), P("tp"), P("fs", "tp"), P("tp"),
        P("tp", "fs"), P("fs"),
    )
    return jax.shard_map(
        functools.partial(layer, mesh.shape["fs"], mesh.shape["tp"]),
        mesh=mesh, in_specs=placed, out_specs=P(("fs", "tp"), None), check_vma=False,
    )
```

time: 657 us -> 326 us (0.50)
  waiting for transfers between devices: 513 us -> 0 us
  Pallas kernels: 0 us -> 308 us
  matrix products: 52.5 us -> 0 us
  blocking collectives: 49.7 us -> 0 us
  between operations: 13.7 us -> 0.03 us
  other arithmetic: 18.4 us -> 9.61 us
    all_gather x8 -> x0, waiting for transfers between devices: 430 us -> none  [the longest x1 99.7 us: local(): lax.all_gather(down_weight.astype(jnp.bfloat16), 'fs', axis=1, tiled=True)]
    pallas_call x0 -> x1, Pallas kernels: none -> 308 us  [layer(): pl.pallas_call(functools.partial(kernel, nf, nt, nz, nx), out_shape=jax.S...]
    reduce_scatter x2 -> x0, waiting for transfers between devices: 83.4 us -> none  [reduce_rows(): lax.psum_scatter(term_fn(jnp.int32(0), lax.axis_size('tp') * local_rows)....]
    dot_general x6 -> x0, matrix products: 52.5 us -> none  [the longest x1 21.4 us: ffn_term(): jnp.dot(hidden, down_whole, preferred_element_type=jnp.float32)]
    all_gather x2 -> x0, blocking collectives: 43.7 us -> none  [the longest x1 22.4 us: local(): lax.all_gather(out_scale, 'fs', axis=0, tiled=True)]
    convert_element_type x10 -> x6, other arithmetic: 15 us -> 5.97 us  [the longest x2 2.27 us: layer(): uv = jnp.concatenate([u_weight.astype(BF), v_weight.astype(BF)], axis=1)]
  transfers between devices with their start and end apart: 10 -> 0, of which waited for: 10 -> 0; matrix products, arithmetic and copies ran while one was open for 7% -> 0% of each run, Pallas kernels for 0% -> 0%
where the time goes in v1:
time: 326 us; the launch traced here: 325 us
  Pallas kernels  308 us (94%)
  other arithmetic  9.61 us (3%)
  local copies, waits for them, and re-layouts  7.09 us (2%)
    pallas_call x1, Pallas kernels, layer(): pl.pallas_call(functools.partial(kernel, nf, nt, nz, nx), out_shape=jax.S...  308 us

profile of v1, /device:TPU:0, one launch (start us, length us, event | category | flops | bytes accessed | tf_op | source)
XLA Modules:
  0.0 324.7 jit_solution(10125562101762349400)
XLA Ops:
  0.0 0.0 copy-start.4
  0.0 0.0 copy-start.3
  0.0 0.8 constant_dynamic-slice_fusion
  0.8 1.3 pad_maximum_fusion.1
  2.0 1.3 broadcast_in_dim.41.gate_scale
  3.3 1.3 broadcast_in_dim.42.up_scale
  4.7 1.5 dynamic-slice_select_fusion.mixers
  6.1 0.7 copy.20
  6.9 0.0 copy-start
  6.9 1.2 convert_element_type.18
  8.1 1.1 convert_element_type.19
  9.1 0.9 pad_maximum_fusion.uv_in
  10.0 0.0 copy-done.4
  10.0 0.0 copy-done.3
  10.0 0.7 multiply_convert_fusion.1.out_in
  10.8 0.0 copy-done
  10.8 1.0 convert_element_type.21.gate_in
  11.7 0.0 copy-done.1
  11.7 1.0 convert_element_type.22.up_in
  12.7 0.7 copy-done.2
  13.4 0.0 copy-done.5
  13.4 1.0 multiply_convert_fusion.down_in
  14.4 307.9 %shard_map.172 = bf16[256,2048]{1,0:T(8,128)(2,1)} custom-call(bf16[256,2048]{1,0:T(8,128)(2,1)} %tokens.1, f32[1,2048]{1,0:T(1,128)} %bitcast.7, f32[1,2048]{1,0:T(1,128)} %bitcast.8, f32[1,1024]{1,0:T(1,128)} %bitcast.6, f32[1,512]{1,0:T(1,128)} %bitcast.9, bf16[2,128,128]{2,1,0:T(8,128)(2,1)} %dynamic-slice_select_fusion.mixers, f32[128,2]{1,0:T(8,128)} %bitcast.5, ...), custom_call_target="tpu_custom_call" | custom-call | tf_op jit(solution)/shard_map/pallas_call | solution.py:343
  322.4 2.3 copy.22
  (4 shorter events, 0.0 us)
Async XLA Ops:
  0.0 10.0 %copy-start.4 = (f32[256]{0:T(256)S(1)}, f32[256]{0:T(256)}, u32[]{:S(2)}) copy-start(f32[256]{0:T(256)} %param.29) | copy-start | bytes 3076
  0.0 10.0 %copy-start.3 = (f32[512,256]{1,0:T(8,128)S(1)}, f32[512,256]{1,0:T(8,128)}, u32[]{:S(2)}) copy-start(f32[512,256]{1,0:T(8,128)} %param.28) | copy-start | bytes 1572868
  6.9 3.9 %copy-start = (f32[256,1536]{1,0:T(8,128)S(1)}, f32[256,1536]{1,0:T(8,128)}, u32[]{:S(2)}) copy-start(f32[256,1536]{1,0:T(8,128)} %param.30) | copy-start | bytes 4718596
  10.0 1.7 copy-start.1
  11.7 1.7 copy-start.2
  11.7 1.7 copy-start.5

commit v2 on v1

--- a/solution.py
+++ b/solution.py
@@ -8,7 +8,9 @@
 
 A_GROUPS = 8
 BLK = 128
-UV, OUT, GATE, UP, DOWN = range(5)
+UV, OUT, GATE, UP, DOWN = (0,), (1,), (2, 3), (4, 5), (6, 7)
+PIECES = 8
+X_FIRST = ()
 BF = jnp.bfloat16
 F32 = jnp.float32
 
@@ -21,10 +23,10 @@
 
 def kernel(
     nf, nt, nz, nx,
-    tokens, mix_gain, ffn_gain, uv_scale, v_gain, mixers, offsets, gate_scale, up_scale,
+    tokens, mix_gain, ffn_gain, u_scale, v_scale, v_gain, mixers, offsets, gate_scale, up_scale,
     uv_in, out_in, gate_in, up_in, down_in,
     result,
-    w_uv, w_out, w_gate, w_up, w_down, rows_all, uvals, vvals, gated, hidden,
+    w_uv, w_out, w_gate, w_up, w_down, rows_all, uvals, vvals, gated, hidden, gates,
     staged, landed, stats, residual,
     own_sem, w_recv, w_send, row_recv, row_send, stat_recv, stat_send, part_recv, part_send,
 ):
@@ -32,19 +34,29 @@
     coord = {"z": fs // nx, "x": fs % nx}
     size = {"z": nz, "x": nx}
     stride = {"z": nx, "x": 1}
-    order = {m: ("z", "x") for m in range(5)}
+    order = {m: ("x", "z") if m in X_FIRST else ("z", "x") for m in range(PIECES)}
     local = tokens.shape[0]
     total = rows_all.shape[0]
     width = tokens.shape[1]
     cols = uvals.shape[1]
-    sources = (uv_in, out_in, gate_in, up_in, down_in)
-    whole = (w_uv, w_out, w_gate, w_up, w_down)
+    table = {}
+    for pieces, source, whole in (
+        (UV, uv_in, w_uv), (OUT, out_in, w_out), (GATE, gate_in, w_gate),
+        (UP, up_in, w_up), (DOWN, down_in, w_down),
+    ):
+        for h, m in enumerate(pieces):
+            table[m] = (source, whole, h, source.shape[0] // len(pieces))
+
+    def shard(m):
+        source, _, h, rows = table[m]
+        return source.at[pl.ds(h * rows, rows)]
 
     def slot(m, s):
-        if m in (OUT, DOWN):
-            return whole[m].at[s]
-        depth = sources[m].shape[0]
-        return whole[m].at[pl.ds(pl.multiple_of(s * depth, depth), depth)]
+        source, whole, h, rows = table[m]
+        if m in OUT + DOWN:
+            return whole.at[s, pl.ds(h * rows, rows)]
+        start = s * source.shape[0] + h * rows
+        return whole.at[pl.ds(pl.multiple_of(start, rows), rows)]
 
     def reaches(axis, d):
         return coord[axis] + d < size[axis] if d > 0 else coord[axis] > 0
@@ -69,35 +81,39 @@
 
         pending.append((allowed, m, s, axis, d))
 
-    def own(m, axis):
-        if size[axis] > 1:
-            for d in (1, -1):
-                send(m, fs, axis, d, fs >= 0)
+    def own(pieces, axis):
+        for m in pieces:
+            if size[axis] > 1:
+                for d in (1, -1):
+                    send(m, fs, axis, d, fs >= 0)
 
     def arrived(m, s, axis, d, valid):
         @pl.when(valid)
         def _():
             copy_of(m, s, axis, -d).wait_recv()
 
-    def first_line(m, then=None):
-        p, q = order[m]
-        for t in range(1, size[p]):
-            for d in (1, -1):
-                at = coord[p] - d * t
-                valid = jnp.logical_and(at >= 0, at < size[p])
-                s = jnp.where(valid, fs - d * t * stride[p], fs)
-                arrived(m, s, p, d, valid)
-                if t < size[p] - 1:
-                    send(m, s, p, d, valid)
-                if size[q] > 1:
-                    for e in (1, -1):
-                        send(m, s, q, e, valid)
-                if then:
-                    pl.when(valid)(functools.partial(then, s))
-
-    def second_line(m, then=None):
-        p, q = order[m]
-        for k in range(size[p]):
+    def first_line(pieces, steps=None):
+        p, q = order[pieces[0]]
+        for t in range(1, size[p]) if steps is None else steps:
+            if t >= size[p]:
+                continue
+            for m in pieces:
+                for d in (1, -1):
+                    at = coord[p] - d * t
+                    valid = jnp.logical_and(at >= 0, at < size[p])
+                    s = jnp.where(valid, fs - d * t * stride[p], fs)
+                    arrived(m, s, p, d, valid)
+                    if t < size[p] - 1:
+                        send(m, s, p, d, valid)
+                    if size[q] > 1:
+                        for e in (1, -1):
+                            send(m, s, q, e, valid)
+
+    def second_line(pieces, steps=None, then=None):
+        p, q = order[pieces[0]]
+        for k in range(size[p]) if steps is None else steps:
+            if k >= size[p]:
+                continue
             for sign in (1, -1) if k else (1,):
                 there = coord[p] + sign * k
                 inside = jnp.logical_and(there >= 0, there < size[p])
@@ -106,16 +122,22 @@
                         at = coord[q] - d * t
                         valid = jnp.logical_and(inside, jnp.logical_and(at >= 0, at < size[q]))
                         s = jnp.where(valid, fs + sign * k * stride[p] - d * t * stride[q], fs)
-                        arrived(m, s, q, d, valid)
-                        if t < size[q] - 1:
-                            send(m, s, q, d, valid)
+                        for m in pieces:
+                            arrived(m, s, q, d, valid)
+                            if t < size[q] - 1:
+                                send(m, s, q, d, valid)
                         if then:
                             pl.when(valid)(functools.partial(then, s))
 
-    mine = [pltpu.make_async_copy(sources[m], slot(m, fs), own_sem.at[m]) for m in range(5)]
+    mine = [pltpu.make_async_copy(shard(m), slot(m, fs), own_sem.at[m]) for m in range(PIECES)]
     for copy in mine:
         copy.start()
-    mine[UV].wait()
+
+    def ready(pieces):
+        for m in pieces:
+            mine[m].wait()
+
+    ready(UV)
     own(UV, "z")
     own(UV, "x")
 
@@ -153,24 +175,25 @@
         def _(i):
             here = pl.ds(pl.multiple_of(i * step, step), step)
             there = pl.ds(pl.multiple_of(tp * local + i * step, step), step)
-            rows_all[there, :] = rms(source[here, :], gain[...])
+            rows_all[there, :] = rms(source[here, :], gain[...][None])
 
     norm_rows(tokens, mix_gain)
     for j in range(1, nt):
         row_copy(0, j, tp).start()
-    mine[OUT].wait()
+    ready(OUT)
     own(OUT, "x")
     own(OUT, "z")
-    mine[GATE].wait()
+    ready(GATE)
     own(GATE, "x")
     first_line(UV)
     own(GATE, "z")
-    mine[UP].wait()
+    ready(UP)
     own(UP, "x")
     second_line(UV)
     for j in range(1, nt):
         row_copy(0, j, peer_of(j)).wait_recv()
 
+    first_line(OUT, (1, 2))
     tile = 256
     stat_rows = BLK
 
@@ -180,7 +203,9 @@
         for c in range(2 * cols // tile):
             at = slice(c * tile, (c + 1) * tile)
             pre = jnp.dot(rows_all[here, :], w_uv[:, at], preferred_element_type=F32)
-            value = jax.nn.gelu(pre * uv_scale[:, at], approximate=True).astype(BF)
+            scale, away = (u_scale, 0) if c * tile < cols else (v_scale, cols)
+            pre = pre * scale[c * tile - away:(c + 1) * tile - away][None]
+            value = jax.nn.gelu(pre, approximate=True).astype(BF)
             if c * tile < cols:
                 uvals[here, at] = value
             else:
@@ -199,14 +224,19 @@
 
     for j in range(1, nt):
         stat_copy(j, tp).start()
-    first_line(OUT)
+    first_line(OUT, range(3, nz))
     own(UP, "z")
-    mine[DOWN].wait()
+    ready(DOWN)
     own(DOWN, "x")
     second_line(OUT)
     for j in range(1, nt):
         stat_copy(j, peer_of(j)).wait_recv()
 
+    causal = (
+        lax.broadcasted_iota(jnp.int32, (BLK, BLK), 0)
+        >= lax.broadcasted_iota(jnp.int32, (BLK, BLK), 1)
+    )
+    groups = A_GROUPS // nt
     group_dim = (cols * nt) // A_GROUPS
 
     @pl.loop(0, total // BLK)
@@ -219,10 +249,12 @@
         average = turned[:, 0:1] / (cols * nt)
         spread = turned[:, 1:2] / (cols * nt) - average * average
         wide = vvals[here, :].astype(F32)
-        normed = ((wide - average) * lax.rsqrt(spread + 1e-05) * v_gain[...]).astype(BF)
+        normed = ((wide - average) * lax.rsqrt(spread + 1e-05) * v_gain[...][None]).astype(BF)
         for g in range(cols // group_dim):
             at = slice(g * group_dim, (g + 1) * group_dim)
-            mixed = jnp.dot(mixers[g], normed[:, at], preferred_element_type=F32)
+            weights = mixers[tp * groups + g].astype(F32)
+            weights = jnp.where(causal, weights, 0.0).astype(BF)
+            mixed = jnp.dot(weights, normed[:, at], preferred_element_type=F32)
             mixed = mixed + offsets[:, g:g + 1]
             gated[here, at] = (uvals[here, at].astype(F32) * mixed).astype(BF)
 
@@ -264,43 +296,56 @@
     norm_rows(residual, ffn_gain)
     for j in range(1, nt):
         row_copy(1, j, tp).start()
+    first_line(UP, (1,))
 
     @pl.loop(0, nf)
     def _(s):
         for j in range(1, nt):
             part_copy(0, j, tp, s).wait_send()
 
-    first_line(UP)
     second_line(GATE)
+    first_line(UP, (2,))
     for j in range(1, nt):
         row_copy(1, j, peer_of(j)).wait_recv()
-    first_line(DOWN)
+    hidden_cols = hidden.shape[1]
+    part = min(512, total)
+
+    def each_tile(body):
+        @pl.loop(0, hidden_cols // tile)
+        def _(c):
+            at = pl.ds(pl.multiple_of(c * tile, tile), tile)
+
+            @pl.loop(0, total // part)
+            def _(i):
+                body(pl.ds(pl.multiple_of(i * part, part), part), at)
+
+    def gate_tile(here, at):
+        gate = jnp.dot(rows_all[here, :], w_gate[:, at], preferred_element_type=F32)
+        gate = gate * gate_scale[at][None]
+        gates[here, at] = gate / (1.0 + jnp.exp(-gate))
+
+    def up_tile(here, at):
+        up = jnp.dot(rows_all[here, :], w_up[:, at], preferred_element_type=F32)
+        hidden[here, at] = (gates[here, at] * (up * up_scale[at][None])).astype(BF)
+
+    each_tile(gate_tile)
+    first_line(UP, range(3, nz))
+    first_line(DOWN, (1,))
     second_line(UP)
-    hidden_cols = hidden.shape[1]
-
-    @pl.loop(0, hidden_cols // tile)
-    def _(c):
-        at = pl.ds(pl.multiple_of(c * tile, tile), tile)
-
-        @pl.loop(0, total // tile)
-        def _(i):
-            here = pl.ds(pl.multiple_of(i * tile, tile), tile)
-            gate = jnp.dot(rows_all[here, :], w_gate[:, at], preferred_element_type=F32)
-            gate = gate * gate_scale[:, at]
-            up = jnp.dot(rows_all[here, :], w_up[:, at], preferred_element_type=F32)
-            up = up * up_scale[:, at]
-            hidden[here, at] = (gate / (1.0 + jnp.exp(-gate)) * up).astype(BF)
+    each_tile(up_tile)
+
+    def down_of(s):
+        product(1, hidden, w_down, s)
 
     for k in range(nz):
+        if k:
+            first_line(DOWN, (k + 1,))
         for sign in (1, -1) if k else (1,):
             there = coord["z"] + sign * k
             inside = jnp.logical_and(there >= 0, there < nz)
-
-            @pl.when(inside)
-            def _():
-                product(1, hidden, w_down, fs + sign * k * nx)
-
-    second_line(DOWN, lambda s: product(1, hidden, w_down, s))
+            pl.when(inside)(functools.partial(down_of, fs + sign * k * nx))
+        second_line(DOWN, (k,), down_of)
+
     collect(1, residual, result)
     for j in range(1, nt):
         row_copy(1, j, tp).wait_send()
@@ -328,12 +373,8 @@
     cols, ff = u_weight.shape[1], gate_weight.shape[1]
     groups = A_GROUPS // nt
     first = lax.axis_index("tp") * groups
-    causal = jnp.tril(jnp.ones((BLK, BLK), dtype=bool))
-    mixers = lax.dynamic_slice_in_dim(spatial_weight, first, groups, 0)
-    mixers = jnp.where(causal[None], mixers, jnp.zeros_like(mixers))
     offsets = lax.dynamic_slice_in_dim(spatial_bias, first, groups, 0).T
     uv = jnp.concatenate([u_weight.astype(BF), v_weight.astype(BF)], axis=1)
-    uv_scale = jnp.concatenate([u_scale, v_scale])[None]
     out = (out_weight * out_scale[None]).astype(BF)
     down = (down_weight * down_scale[None]).astype(BF)
     block = out.shape[1]
@@ -343,7 +384,7 @@
     return pl.pallas_call(
         functools.partial(kernel, nf, nt, nz, nx),
         out_shape=jax.ShapeDtypeStruct((local, width), BF),
-        in_specs=[vmem] * 9 + [hbm] * 5,
+        in_specs=[vmem] * 10 + [hbm] * 5,
         out_specs=vmem,
         scratch_shapes=[
             pltpu.VMEM((width, 2 * cols), BF),
@@ -356,11 +397,12 @@
             pltpu.VMEM((total, cols), BF),
             pltpu.VMEM((total, cols), BF),
             pltpu.VMEM((total, ff), BF),
+            pltpu.VMEM((total, ff), F32),
             pltpu.VMEM((nf, total, block), BF),
             pltpu.VMEM((nt, nf, local, block), BF),
             pltpu.VMEM((nt, 8, total), F32),
             pltpu.VMEM((local, width), BF),
-            dma((5,)), dma((5, nf)), dma((5, nf, 4)),
+            dma((PIECES,)), dma((PIECES, nf)), dma((PIECES, nf, 4)),
             dma((2, nt)), dma((2, nt)), dma((nt,)), dma((nt,)),
             dma((2, nt, nf)), dma((2, nt, nf)),
         ],
@@ -368,8 +410,8 @@
             has_side_effects=True, vmem_limit_bytes=67043328
         ),
     )(
-        tokens, mix_gain[None], ffn_gain[None], uv_scale, v_gain[None], mixers, offsets,
-        gate_scale[None], up_scale[None],
+        tokens, mix_gain, ffn_gain, u_scale, v_scale, v_gain, spatial_weight, offsets,
+        gate_scale, up_scale,
         uv, out, gate_weight.astype(BF), up_weight.astype(BF), down,
     )
 

time: 326 us -> 307 us (0.942)
  Pallas kernels: 308 us -> 292 us
    pallas_call x1, Pallas kernels: 308 us -> 292 us  [layer(): pl.pallas_call(functools.partial(kernel, nf, nt, nz, nx), out_shape=jax.S...]
where the time goes in v2:
time: 307 us; the launch traced here: 304 us
  Pallas kernels  292 us (95%)
  other arithmetic  6.84 us (2%)
  local copies, waits for them, and re-layouts  4.5 us (1%)
    pallas_call x1, Pallas kernels, layer(): pl.pallas_call(functools.partial(kernel, nf, nt, nz, nx), out_shape=jax.S...  292 us

profile of v2, /device:TPU:0, one launch (start us, length us, event | category | flops | bytes accessed | tf_op | source)
XLA Modules:
  0.0 303.7 jit_solution(16093585197292172584)
XLA Ops:
  0.0 0.0 copy-start.4
  0.0 0.0 copy-start.3
  0.0 0.8 constant_dynamic-slice_fusion
  0.8 0.7 copy.20
  1.5 0.0 copy-start
  1.5 1.2 convert_element_type.18
  2.7 1.1 convert_element_type.19
  3.8 0.9 pad_maximum_fusion.uv_in
  4.6 0.0 copy-done.4
  4.6 0.0 copy-done.3
  4.6 0.0 copy-start.1
  4.6 0.7 multiply_convert_fusion.1.out_in
  5.4 0.0 copy-done
  5.4 1.0 convert_element_type.21.gate_in
  6.3 0.0 copy-done.1
  6.4 0.0 copy-start.2
  6.4 0.0 copy-start.5
  6.4 1.0 convert_element_type.22.up_in
  7.4 0.7 copy-done.2
  8.0 0.0 copy-done.5
  8.0 1.0 multiply_convert_fusion.down_in
  9.0 292.4 %shard_map.172 = bf16[256,2048]{1,0:T(8,128)(2,1)} custom-call(bf16[256,2048]{1,0:T(8,128)(2,1)} %tokens.1, f32[2048]{0:T(1024)} %mix_gain.1, f32[2048]{0:T(1024)} %ffn_gain.1, f32[512]{0:T(512)} %u_scale.1, f32[512]{0:T(512)} %v_scale.1, f32[512]{0:T(512)} %v_gain.1, bf16[8,128,128]{2,1,0:T(8,128)(2,1)} %mixers.1, f32[128,2]{1,0:T(8,128)} %bitcast.1, ...), custom_call_target="tpu_custom_call" | custom-call | tf_op jit(solution)/shard_map/pallas_call | solution.py:384
  301.4 2.3 copy.22
Async XLA Ops:
  0.0 4.6 %copy-start.4 = (f32[256]{0:T(256)S(1)}, f32[256]{0:T(256)}, u32[]{:S(2)}) copy-start(f32[256]{0:T(256)} %param.29) | copy-start | bytes 3076
  0.0 4.6 %copy-start.3 = (f32[512,256]{1,0:T(8,128)S(1)}, f32[512,256]{1,0:T(8,128)}, u32[]{:S(2)}) copy-start(f32[512,256]{1,0:T(8,128)} %param.28) | copy-start | bytes 1572868
  1.5 3.9 %copy-start = (f32[256,1536]{1,0:T(8,128)S(1)}, f32[256,1536]{1,0:T(8,128)}, u32[]{:S(2)}) copy-start(f32[256,1536]{1,0:T(8,128)} %param.30) | copy-start | bytes 4718596
  4.6 1.7 copy-start.1
  6.4 1.7 copy-start.2
  6.4 1.7 copy-start.5
